TPU v7x, 32 devices: a whole 2x2x4 slice. The times are simulated.
32 devices in a mesh: sp: 8 (over z, x), tp: 4 (over y, core).
Axes of the slice: x: 2, y: 2, z: 4, core: 2. Of those that a mesh axis runs over, the one named last changes fastest.
Arguments:
- residual: bfloat16 [1024, 2048], P(('sp', 'tp')), may hold values from -20 to 20
- query_small: bfloat16 [1024, 384], P('sp', 'tp'), may hold values from -12 to 12
- query_large: bfloat16 [1024, 640], P('sp', 'tp'), may hold values from -12 to 12
- latent: bfloat16 [1024, 512], P('sp'), may hold values from -30 to 30
- rotary_key: bfloat16 [1024, 32], P('sp'), may hold values from -16 to 16
- latent_gain: float32 [512], replicated, may hold values from 0.1 to 1.9
- small_keys: bfloat16 [512, 256], P(None, 'tp'), may hold values from -0.25 to 0.25
- small_values: bfloat16 [512, 256], P(None, 'tp'), may hold values from -0.25 to 0.25
- large_keys: bfloat16 [512, 512], P(None, 'tp'), may hold values from -0.25 to 0.25
- large_values: bfloat16 [512, 512], P(None, 'tp'), may hold values from -0.25 to 0.25
- small_output: bfloat16 [256, 2048], P('tp'), may hold values from -0.21875 to 0.21875
- large_output: bfloat16 [512, 2048], P('tp'), may hold values from -0.21875 to 0.21875
- ffn_gain: float32 [2048], replicated, may hold values from 0.1 to 1.9
- gate_weights: bfloat16 [8, 2048, 2048], P('sp', None, 'tp'), may hold values from -2 to 2
- up_weights: bfloat16 [8, 2048, 2048], P('sp', None, 'tp'), may hold values from -2 to 2
- down_weights: bfloat16 [8, 2048, 2048], P('sp', 'tp'), may hold values from -0.046875 to 0.046875
- routing: int32 [1024, 2], P(('sp', 'tp')), may hold values from 0 to 7, all different within a row; in each aligned block of 32 rows (0 to 31, 32 to 63, ...) at most 16 rows name the same one
- route_weight: float32 [1024, 2], P(('sp', 'tp')), may hold values from 0.2 to 1
Outputs:
- output: bfloat16 [1024, 2048], P(('sp', 'tp'))
Inputs may be any that keep to these rules, and one draw needn't show every extreme that they name: `routing`: each row names 2 different experts. Within the rows of one device (aligned blocks of 32 rows) no expert is named by more than 16 rows, and in every draw some block has an expert named by exactly 16 rows.
All inputs are finite; a program needn't handle non-finite values.
Results may differ from a plain program's by a relative error of at most 0.018.
Values may be sent and summed in bfloat16 or wider, within the bound.
A program may use at most 128 MiB of HBM per device.

v0:
```python
import jax
import jax.numpy as jnp
from jax import lax
from jax.sharding import PartitionSpec as P

NOPE_S = 64
NOPE_L = 128
ROPE = 32
TOPK = 2


eps = 1e-06
clamp_limit = 7.0
glu_alpha = 1.702
rope_base = 10000.0
masked_score = -1e30


def rope_tables(row_count, first_pos):
    half_size = ROPE // 2
    frequencies = jnp.power(rope_base, -jnp.arange(half_size, dtype=jnp.float32) * (2.0 / ROPE))
    places = (first_pos + jnp.arange(row_count, dtype=jnp.int32)).astype(jnp.float32)
    angles = places[:, None] * frequencies[None, :]
    return (jnp.cos(angles), jnp.sin(angles))


def rotate(values_in, cos_vals, sin_vals):
    front_half, back_half = jnp.split(values_in, 2, axis=-1)
    return jnp.concatenate(
        [
            front_half * cos_vals - back_half * sin_vals,
            back_half * cos_vals + front_half * sin_vals,
        ],
        axis=-1,
    )


def rms_scaled(values_in, gain):
    widened = values_in.astype(jnp.float32)
    return widened * lax.rsqrt(jnp.mean(widened * widened, axis=-1, keepdims=True) + eps) * gain


def turn_queries(query, nope, cos_vals, sin_vals):
    width = nope + ROPE
    shaped = query.reshape(query.shape[0], query.shape[1] // width, width)
    turned = rotate(
        shaped[:, :, nope:].astype(jnp.float32), cos_vals[:, None, :], sin_vals[:, None, :]
    )
    return jnp.concatenate([shaped[:, :, :nope], turned.astype(jnp.bfloat16)], axis=2)


def clamped(gate_pre, up_pre):
    limited = jnp.minimum(gate_pre, clamp_limit)
    linear = jnp.clip(up_pre, -clamp_limit, clamp_limit)
    return limited * jax.nn.sigmoid(glu_alpha * limited) * (linear + 1.0)


def make_keys(latent_rows, raw_rotary, first_pos, latent_gain, projections):
    normed_latent = rms_scaled(latent_rows, latent_gain).astype(jnp.bfloat16)
    projected = tuple(
        (
            jnp.dot(normed_latent, weight, preferred_element_type=jnp.float32).astype(jnp.bfloat16)
            for weight in projections
        )
    )
    cos_vals, sin_vals = rope_tables(latent_rows.shape[0], first_pos)
    turned = rotate(raw_rotary.astype(jnp.float32), cos_vals, sin_vals).astype(jnp.bfloat16)
    return projected + (turned,)


def empty_state(query, values_in):
    head_count = query.shape[1]
    row_count = query.shape[0]
    value_size = values_in.shape[1] // head_count
    return (
        jnp.full((head_count, row_count), masked_score, jnp.float32),
        jnp.zeros((head_count, row_count), jnp.float32),
        jnp.zeros((row_count, head_count, value_size), jnp.float32),
    )


def update(state_now, query, keys_in, values_in, rotary, nope, allowed):
    running_max, weight_sum, weighted = state_now
    head_count = query.shape[1]
    span_rows = rotary.shape[0]
    key_heads = keys_in.reshape(span_rows, head_count, nope)
    value_heads = values_in.reshape(span_rows, head_count, -1)
    scores = jnp.einsum(
        "rhd,khd->hrk", query[:, :, :nope], key_heads, preferred_element_type=jnp.float32
    )
    scores = scores + jnp.einsum(
        "rhd,kd->hrk", query[:, :, nope:], rotary, preferred_element_type=jnp.float32
    )
    scores = jnp.where(allowed[None], scores * (nope + ROPE) ** (-0.5), masked_score)
    new_max = jnp.maximum(running_max, jnp.max(scores, axis=2))
    weights = jnp.where(allowed[None], jnp.exp(scores - new_max[:, :, None]), 0.0)
    rescale = jnp.exp(running_max - new_max)
    weight_sum = jnp.sum(weights, axis=2)
    weighted = weighted * rescale.T[:, :, None] + jnp.einsum(
        "hrk,khd->rhd",
        weights.astype(jnp.bfloat16),
        value_heads,
        preferred_element_type=jnp.float32,
    )
    return (new_max, weight_sum, weighted)


def finish(state_end, row_count):
    running_max, weight_sum, weighted = state_end
    return (weighted / weight_sum.T[:, :, None]).reshape(row_count, -1).astype(jnp.bfloat16)


def on_device(
    residual,
    query_small,
    query_large,
    latent,
    rotary_key,
    latent_gain,
    small_keys,
    small_values,
    large_keys,
    large_values,
    small_output,
    large_output,
    ffn_gain,
    gate_weights,
    up_weights,
    down_weights,
    routing,
    route_weight,
):
    row_count = latent.shape[0]
    first_pos = lax.axis_index("sp") * row_count
    cos_vals, sin_vals = rope_tables(row_count, first_pos)
    small_query = turn_queries(query_small, NOPE_S, cos_vals, sin_vals)
    large_query = turn_queries(query_large, NOPE_L, cos_vals, sin_vals)
    query_pos = first_pos + jnp.arange(row_count, dtype=jnp.int32)
    last_pos = first_pos + row_count - 1
    projections = (small_keys, small_values, large_keys, large_values)
    initial = (empty_state(small_query, small_values), empty_state(large_query, large_values))

    def from_latent(key_set, offset):
        return make_keys(key_set[0], key_set[1], offset, latent_gain, projections)

    key_set = (
        lax.all_gather(latent, "sp", axis=0, tiled=True),
        lax.all_gather(rotary_key, "sp", axis=0, tiled=True),
    )
    offset = jnp.int32(0)
    span_rows = key_set[0].shape[0]
    allowed = jnp.arange(span_rows, dtype=jnp.int32)[None, :] <= query_pos[:, None]

    def live(inner):
        ready = from_latent(key_set, offset)
        return (
            update(inner[0], small_query, ready[0], ready[1], ready[4], NOPE_S, allowed),
            update(inner[1], large_query, ready[2], ready[3], ready[4], NOPE_L, allowed),
        )

    def keep_state(inner):
        return inner

    state_end = lax.cond(offset <= last_pos, live, keep_state, initial)
    small_heads = finish(state_end[0], row_count)
    large_heads = finish(state_end[1], row_count)
    tok_count = row_count // lax.axis_size("tp")
    summed = lax.psum_scatter(
        (
            jnp.dot(small_heads, small_output, preferred_element_type=jnp.float32)
            + jnp.dot(large_heads, large_output, preferred_element_type=jnp.float32)
        ).astype(jnp.bfloat16),
        "tp",
        scatter_dimension=0,
        tiled=True,
    )
    attention = lax.optimization_barrier(summed).astype(jnp.float32)
    middle = lax.optimization_barrier(
        (residual.astype(jnp.float32) + attention).astype(jnp.bfloat16)
    )
    normed = rms_scaled(middle, ffn_gain).astype(jnp.bfloat16)
    local_experts = gate_weights.shape[0]
    expert_count = local_experts * lax.axis_size("sp")
    capacity = max(2, 2 * TOPK * tok_count // expert_count)
    assigned = routing.reshape(-1)
    onehot = (assigned[:, None] == jnp.arange(expert_count, dtype=jnp.int32)[None, :]).astype(
        jnp.int32
    )
    slot_index = jnp.sum((jnp.cumsum(onehot, axis=0) - onehot) * onehot, axis=1)
    places = assigned * capacity + slot_index
    pick_table = (
        places[:, None] == jnp.arange(expert_count * capacity, dtype=jnp.int32)[None, :]
    ).astype(jnp.bfloat16)
    send_table = jnp.sum(pick_table.reshape(tok_count, TOPK, -1), axis=1)
    outgoing = lax.dot_general(
        send_table, normed, (((0,), (0,)), ((), ())), preferred_element_type=jnp.float32
    )
    outgoing = outgoing.astype(jnp.bfloat16).reshape(expert_count, capacity, -1)
    shard_piece = lax.all_gather(
        lax.all_to_all(outgoing, "sp", split_axis=0, concat_axis=0, tiled=True),
        "tp",
        axis=0,
        tiled=True,
    )
    grouped = shard_piece.reshape(-1, local_experts, shard_piece.shape[1], shard_piece.shape[2])
    gate_pre = jnp.einsum(
        "secd,edf->secf", grouped, gate_weights, preferred_element_type=jnp.float32
    )
    up_pre = jnp.einsum("secd,edf->secf", grouped, up_weights, preferred_element_type=jnp.float32)
    hidden = clamped(gate_pre, up_pre).astype(jnp.bfloat16)
    result = jnp.einsum("secf,efd->secd", hidden, down_weights, preferred_element_type=jnp.float32)
    partials = result.reshape(shard_piece.shape[0], shard_piece.shape[1], -1)
    combined = lax.psum_scatter(
        partials.astype(jnp.bfloat16), "tp", scatter_dimension=0, tiled=True
    )
    returned = lax.all_to_all(combined, "sp", split_axis=0, concat_axis=0, tiled=True)
    picked = jnp.dot(
        pick_table,
        returned.reshape(expert_count * capacity, -1),
        preferred_element_type=jnp.float32,
    )
    mixed = jnp.sum(route_weight[:, :, None] * picked.reshape(tok_count, TOPK, -1), axis=1)
    return (middle.astype(jnp.float32) + mixed).astype(jnp.bfloat16)


def solution(mesh):
    return jax.shard_map(
        on_device,
        mesh=mesh,
        in_specs=(
            P(("sp", "tp"), None),
            P("sp", "tp"),
            P("sp", "tp"),
            P("sp", None),
            P("sp", None),
            P(),
            P(None, "tp"),
            P(None, "tp"),
            P(None, "tp"),
            P(None, "tp"),
            P("tp", None),
            P("tp", None),
            P(),
            P("sp", None, "tp"),
            P("sp", None, "tp"),
            P("sp", "tp", None),
            P(("sp", "tp"), None),
            P(("sp", "tp"), None),
        ),
        out_specs=P(("sp", "tp"), None),
        check_vma=False,
    )
```

profile of v0, /device:TPU:0, one launch (start us, length us, event | category | flops | bytes accessed | tf_op | source)
XLA Modules:
  0.0 206.3 jit_solution(8740925484873933888)
XLA Ops:
  6.5 0.7 all-gather.3.cloned.1.call-update
  7.3 0.0 reduce-scatter.3.cloned.1.call-start
  7.3 28.0 %all_gather.10 = bf16[1024,32]{0,1:T(8,128)(2,1)S(1)} all-gather(bf16[128,32]{0,1:T(8,128)(2,1)} %param.24), channel_id=1, replica_groups=mesh['sp'=8,'tp'=4] {'sp'}, dimensions={0}, use_global_device_ids=true | all-gather | bytes 73728 | tf_op jit(solution)/shard_map/all_gather | solution.py:148
  35.3 0.7 slice_convert_fusion.1
  36.0 0.7 slice_convert_fusion
  36.7 0.1 fusion.120
  36.9 16.0 %all-gather.3.cloned.1.call-done = bf16[1024,512]{1,0:T(8,128)(2,1)} async-done(((bf16[128,512]{1,0:T(8,128)(2,1)}), bf16[1024,512]{1,0:T(8,128)(2,1)}) %all-gather.3.cloned.1.call-update) | async-done | bytes 1048592 | tf_op jit(solution)/shard_map/all_gather | solution.py:147
  52.9 19.2 %conditional.1 = (f32[1,128]{1,0:T(1,128)}, f32[128,1,64]{0,2,1:T(8,128)}, f32[1,128]{1,0:T(1,128)}, f32[128,1,128]{0,2,1:T(8,128)}) conditional(s32[]{:T(128)} %convert_element_type.128, () %tuple.13, (s32[]{:T(128)}, s32[128,1]{0,1:T(1,128)S(1)}, s32[128,1024]{0,1:T(8,128)S(1)}, bf16[1024,512]{1,0:T(8,128)(2,1)}, f32[512]{0:T(512)}, ...), branch_computations={%region_0.0_spmd, %region_1.7_spmd} | conditional | flops 533801376 | bytes 19827048 | solution.py:164
  52.9 1.5 fusion
  54.5 0.6 add_rsqrt_fusion
  55.1 1.5 copy.58
  56.6 0.7 broadcast_compare_fusion
  57.3 0.3 fusion.34
  57.7 1.1 convolution_bitcast_fusion
  58.8 2.2 %fusion.127 = (f32[128]{0:T(128)S(1)}, f32[1,128,1024]{1,2,0:T(8,128)S(1)}) fusion(f32[1,128,1024]{1,2,0:T(8,128)} %convolution_bitcast_fusion, bf16[128,1,160]{2,0,1:T(8,128)(2,1)} %copy.58, bf16[512,128]{1,0:T(8,128)(2,1)} %get-tuple-element.70, bf16[1024,512]{1,0:T(8,128)(2,1)} %get-tuple-element.43, f32[512]{0:T(512)} %get-tuple-element.67, ...), kind=kOutput, calls=%fused_computation.146 | convolution fusion | flops 170524544 | bytes 2398720 | tf_op jit(solution)/shard_map/cond/branch_1_fun/rhd,khd->hrk/dot_general | solution.py:88
  60.9 1.1 convolution_bitcast_fusion.1
  62.0 3.0 %fusion.130 = (f32[128]{0:T(128)S(1)}, f32[1,128,1024]{1,2,0:T(8,128)}) fusion(f32[1,128,1024]{1,2,0:T(8,128)} %convolution_bitcast_fusion.1, bf16[128,1,96]{0,2,1:T(8,128)(2,1)S(1)} %copy-done.8, bf16[512,64]{0,1:T(8,128)(2,1)} %get-tuple-element.133, bf16[1024,512]{1,0:T(8,128)(2,1)} %get-tuple-element.43, f32[512]{0:T(512)S(1)} %copy-done.12, ...), kind=kOutput, calls=%fused_computation.147 | convolution fusion | flops 86572928 | bytes 2316800 | tf_op jit(solution)/shard_map/cond/branch_1_fun/rhd,khd->hrk/dot_general | solution.py:88
  65.1 1.8 fusion.20
  66.9 2.8 %fusion.16 = f32[128,1,64]{0,2,1:T(8,128)} fusion(bf16[512,64]{0,1:T(8,128)(2,1)} %get-tuple-element.137, f32[1,128,1024]{1,2,0:T(8,128)} %get-tuple-element.153, pred[128,1024]{0,1:T(32,128)(4,1)} %broadcast_compare_fusion, f32[128]{0:T(128)S(1)} %get-tuple-element.154, f32[128]{0:T(128)S(1)} %get-tuple-element.155, ...), kind=kOutput, calls=%fused_computation.26 | convolution fusion | flops 86450176 | bytes 1809408 | tf_op jit(solution)/shard_map/cond/branch_1_fun/hrk,khd->rhd/dot_general | solution.py:99
  69.7 2.4 %fusion.13 = f32[128,1,128]{0,2,1:T(8,128)} fusion(bf16[512,128]{1,0:T(8,128)(2,1)} %get-tuple-element.71, f32[1,128,1024]{1,2,0:T(8,128)} %copy-done.2, pred[128,1024]{0,1:T(32,128)(4,1)} %broadcast_compare_fusion, f32[128]{0:T(128)S(1)} %get-tuple-element.147, f32[128]{0:T(128)S(1)} %get-tuple-element.146, bf16[1024,512]{1,0:T(8,128)(2,1)S(1)} %copy-done.1, ...), kind=kOutput, calls=%fused_computation.23 | convolution fusion | flops 170409984 | bytes 1907712 | tf_op jit(solution)/shard_map/cond/branch_1_fun/hrk,khd->rhd/dot_general | solution.py:99
  72.1 0.0 copy-start.5
  72.1 1.1 fusion.104
  73.3 2.2 %fusion.53 = bf16[128,2048]{1,0:T(8,128)(2,1)} fusion(f32[128,2048]{1,0:T(8,128)S(1)} %fusion.104, bf16[128,2048]{1,0:T(8,128)(2,1)} %param.31, f32[128,1,128]{0,2,1:T(8,128)} %get-tuple-element.60, f32[128]{0:T(128)} %bitcast.26), kind=kOutput, calls=%fused_computation.70 | convolution fusion | flops 67665920 | bytes 2163200 | tf_op jit(solution)/shard_map/dot_general | solution.py:171
  75.5 0.0 reduce-scatter.3.cloned.1.call-update
  75.5 0.0 all-gather.5.cloned.1.call-start
  75.6 0.1 copy.59
  75.6 0.1 eq.51
  75.8 0.1 fusion.99
  75.8 0.1 reduce_window_sum.11
  75.9 0.2 select_reduce_fusion
  76.1 0.1 reduce_sum.73
  76.2 0.1 copy.60
  76.3 0.1 fusion.103
  76.4 19.7 %reduce-scatter.3.cloned.1.call-done = bf16[32,2048]{1,0:T(8,128)(2,1)} async-done(((bf16[128,2048]{1,0:T(8,128)(2,1)}), bf16[32,2048]{1,0:T(8,128)(2,1)}) %reduce-scatter.3.cloned.1.call-update) | async-done | bytes 131088 | tf_op jit(solution)/shard_map/reduce_scatter | solution.py:168
  96.1 0.9 add_convert_fusion
  97.0 0.1 fusion.91
  97.2 0.3 convolution_convert_fusion.5
  97.5 19.8 %all_to_all.10 = bf16[8,16,2048]{2,1,0:T(8,128)(2,1)} all-to-all(bf16[8,16,2048]{2,1,0:T(8,128)(2,1)S(1)} %bitcast.170), channel_id=1, replica_groups=mesh['sp'=8,'tp'=4] {'sp'}, dimensions={0} | all-to-all | bytes 1048576 | tf_op jit(solution)/shard_map/all_to_all | solution.py:200
  117.3 0.0 all-gather.5.cloned.1.call-update
  117.3 0.0 reduce-scatter.5.cloned.1.call-start
  117.4 20.8 %all-gather.5.cloned.1.call-done = bf16[32,16,2048]{2,1,0:T(8,128)(2,1)} async-done(((bf16[8,16,2048]{2,1,0:T(8,128)(2,1)}), bf16[32,16,2048]{2,1,0:T(8,128)(2,1)}) %all-gather.5.cloned.1.call-update) | async-done | bytes 2097168 | tf_op jit(solution)/shard_map/all_gather | solution.py:199
  138.1 3.5 %fusion.62 = f32[32,1,16,512]{3,2,0,1:T(8,128)S(1)} fusion(bf16[32,16,2048]{2,1,0:T(8,128)(2,1)} %all-gather.5.cloned.1.call-done, bf16[1,2048,512]{2,1,0:T(8,128)(2,1)} %param.33), kind=kOutput, calls=%fused_computation.79 | convolution fusion | flops 1074003968 | bytes 5242880 | tf_op jit(solution)/shard_map/secd,edf->secf/dot_general | solution.py:206
  141.6 6.0 %convolution_convert_fusion.4 = bf16[32,16,2048]{2,1,0:T(8,128)(2,1)} fusion(bf16[1,512,2048]{2,1,0:T(8,128)(2,1)S(1)} %copy-done, bf16[32,16,2048]{2,1,0:T(8,128)(2,1)} %all-gather.5.cloned.1.call-done, bf16[1,2048,512]{2,1,0:T(8,128)(2,1)} %param.34, f32[32,1,16,512]{3,2,0,1:T(8,128)S(1)} %fusion.62), kind=kOutput, calls=%fused_computation.68 | convolution fusion | flops 2150891520 | bytes 9437184 | tf_op jit(solution)/shard_map/secf,efd->secd/dot_general | solution.py:211
  147.6 0.0 reduce-scatter.5.cloned.1.call-update
  147.7 31.3 %reduce-scatter.5.cloned.1.call-done = bf16[8,16,2048]{2,1,0:T(8,128)(2,1)} async-done(((bf16[32,16,2048]{2,1,0:T(8,128)(2,1)}), bf16[8,16,2048]{2,1,0:T(8,128)(2,1)}) %reduce-scatter.5.cloned.1.call-update) | async-done | bytes 524304 | tf_op jit(solution)/shard_map/reduce_scatter | solution.py:213
  179.0 19.9 %all_to_all.11 = bf16[8,16,2048]{2,1,0:T(8,128)(2,1)S(1)} all-to-all(bf16[8,16,2048]{2,1,0:T(8,128)(2,1)} %reduce-scatter.5.cloned.1.call-done), channel_id=1, replica_groups=mesh['sp'=8,'tp'=4] {'sp'}, dimensions={0} | all-to-all | bytes 1048576 | tf_op jit(solution)/shard_map/all_to_all | solution.py:216
  198.8 0.3 fusion.83
  199.1 0.7 fusion.94
  (38 shorter events, 0.2 us)
Async XLA Ops:
  6.5 135.1 %copy-start = (bf16[1,512,2048]{2,1,0:T(8,128)(2,1)S(1)}, bf16[1,512,2048]{2,1,0:T(8,128)(2,1)}, u32[]{:S(2)}) copy-start(bf16[1,512,2048]{2,1,0:T(8,128)(2,1)} %param.35) | copy-start | bytes 6291460
  6.5 46.3 %all-gather.3.cloned.1.call-start = ((), (), s32[]{:S(2)}) async-start(), calls=%async_computation.4 | async-start | bytes 1179648 | tf_op jit(solution)/shard_map/all_gather | solution.py:147
  7.3 88.8 %reduce-scatter.3.cloned.1.call-start = ((), (), s32[]{:S(2)}) async-start(), calls=%async_computation.5 | async-start | bytes 655360 | tf_op jit(solution)/shard_map/reduce_scatter | solution.py:168
  52.9 19.3 %copy-start.3 = (bf16[64,2048]{1,0:T(8,128)(2,1)S(1)}, bf16[64,2048]{1,0:T(8,128)(2,1)}, u32[]{:S(2)}) copy-start(bf16[64,2048]{1,0:T(8,128)(2,1)} %param.30) | copy-start | bytes 786436
  52.9 4.8 %copy-start.9 = (s32[128]{0:T(128)}, s32[128]{0:T(128)S(1)}, u32[]{:S(2)}) copy-start(s32[128]{0:T(128)S(1)} %add_bitcast_fusion) | copy-start | bytes 1540 | tf_op jit(solution)/shard_map/cond
  57.6 4.4 %copy-start.7 = (f32[1024]{0:T(1024)S(1)}, f32[1024]{0:T(1024)}, u32[]{:S(2)}) copy-start(f32[1024]{0:T(1024)} %add_rsqrt_fusion) | copy-start | bytes 12292 | tf_op jit(solution)/shard_map/cond
  57.6 4.4 %copy-start.8 = (bf16[128,1,96]{0,2,1:T(8,128)(2,1)S(1)}, bf16[128,1,96]{0,2,1:T(8,128)(2,1)}, u32[]{:S(2)}) copy-start(bf16[128,1,96]{0,2,1:T(8,128)(2,1)} %get-tuple-element.46) | copy-start | bytes 73732 | tf_op jit(solution)/shard_map/cond
  57.7 4.4 %copy-start.12 = (f32[512]{0:T(512)S(1)}, f32[512]{0:T(512)}, u32[]{:S(2)}) copy-start(f32[512]{0:T(512)} %get-tuple-element.67) | copy-start | bytes 6148 | tf_op jit(solution)/shard_map/cond
  60.9 4.1 %copy-start.2 = (f32[1,128,1024]{1,2,0:T(8,128)}, f32[1,128,1024]{1,2,0:T(8,128)S(1)}, u32[]{:S(2)}) copy-start(f32[1,128,1024]{1,2,0:T(8,128)S(1)} %get-tuple-element.151) | copy-start | bytes 1572868 | tf_op jit(solution)/shard_map/cond
  60.9 4.1 %copy-start.10 = (s32[128]{0:T(128)S(1)}, s32[128]{0:T(128)}, u32[]{:S(2)}) copy-start(s32[128]{0:T(128)} %copy-done.9) | copy-start | bytes 1540 | tf_op jit(solution)/shard_map/cond
  66.9 2.8 %copy-start.1 = (bf16[1024,512]{1,0:T(8,128)(2,1)S(1)}, bf16[1024,512]{1,0:T(8,128)(2,1)}, u32[]{:S(2)}) copy-start(bf16[1024,512]{1,0:T(8,128)(2,1)} %get-tuple-element.43) | copy-start | bytes 3145732 | tf_op jit(solution)/shard_map/cond
  72.1 3.4 %copy-start.6 = (s32[32,2]{0,1:T(2,128)S(1)}, s32[32,2]{0,1:T(2,128)}, u32[]{:S(2)}) copy-start(s32[32,2]{0,1:T(2,128)} %param.36) | copy-start | bytes 772
  72.1 23.9 %copy-start.4 = (bf16[32,2048]{1,0:T(8,128)(2,1)S(1)}, bf16[32,2048]{1,0:T(8,128)(2,1)}, u32[]{:S(2)}) copy-start(bf16[32,2048]{1,0:T(8,128)(2,1)} %param.20) | copy-start | bytes 393220
  72.1 25.0 %copy-start.5 = (f32[2048]{0:T(1024)S(1)}, f32[2048]{0:T(1024)}, u32[]{:S(2)}) copy-start(f32[2048]{0:T(1024)} %param.32) | copy-start | bytes 24580
  75.5 62.6 %all-gather.5.cloned.1.call-start = ((), (), s32[]{:S(2)}) async-start(), calls=%async_computation.6 | async-start | bytes 2621440 | tf_op jit(solution)/shard_map/all_gather | solution.py:199
  117.3 61.6 %reduce-scatter.5.cloned.1.call-start = ((), (), s32[]{:S(2)}) async-start(), calls=%async_computation.7 | async-start | bytes 2621440 | tf_op jit(solution)/shard_map/reduce_scatter | solution.py:213
  147.6 51.2 %copy-start.11 = (f32[32,2]{0,1:T(2,128)S(1)}, f32[32,2]{0,1:T(2,128)}, u32[]{:S(2)}) copy-start(f32[32,2]{0,1:T(2,128)} %param.37) | copy-start | bytes 772
Sparse Core Ops, SparseCore 0:
  9.5 43.3 all-gather.2
  75.6 20.4 reduce-scatter.2
  117.5 20.6 all-gather.4
  147.8 31.1 reduce-scatter.4
where the time goes:
time: 207 us; the launch traced here: 206 us
  waiting for transfers between devices  88.5 us (43%)
  blocking collectives  67.6 us (33%)
  matrix products  26 us (13%)
  between operations  13.2 us (6%)
  other arithmetic  8.79 us (4%)
    reduce_scatter x1, waiting for transfers between devices, on_device(): lax.psum_scatter(partials.astype(jnp.bfloat16), 'tp', scatter_dimension=0...  31.3 us
    all_gather x1, blocking collectives, on_device(): lax.all_gather(rotary_key, 'sp', axis=0, tiled=True)  28 us
    all_gather x1, waiting for transfers between devices, on_device(): lax.all_gather(lax.all_to_all(outgoing, 'sp', split_axis=0, concat_axis=0...  20.8 us
    all_to_all x1, blocking collectives, on_device(): lax.all_to_all(combined, 'sp', split_axis=0, concat_axis=0, tiled=True)  19.9 us
    all_to_all x1, blocking collectives, on_device(): lax.all_to_all(outgoing, 'sp', split_axis=0, concat_axis=0, tiled=True)  19.8 us
    reduce_scatter x1, waiting for transfers between devices, on_device(): lax.psum_scatter((jnp.dot(small_heads, small_output, preferred_element_ty...  19.7 us
    all_gather x1, waiting for transfers between devices, on_device(): lax.all_gather(latent, 'sp', axis=0, tiled=True)  16 us
    dot_general x1, matrix products, on_device(): jnp.einsum('secf,efd->secd', hidden, down_weights, preferred_element_type...  6.02 us
  transfers between devices with their start and end apart: 4, of which 4 were waited for; matrix products, arithmetic and copies ran while one was open for 1% of the time, Pallas kernels for 0%

commit v1 on v0

--- a/solution.py
+++ b/solution.py
@@ -1,6 +1,10 @@
+import functools
+
 import jax
 import jax.numpy as jnp
 from jax import lax
+from jax.experimental import pallas as pl
+from jax.experimental.pallas import tpu as pltpu
 from jax.sharding import PartitionSpec as P
 
 NOPE_S = 64
@@ -223,9 +227,584 @@
     return (middle.astype(jnp.float32) + mixed).astype(jnp.bfloat16)
 
 
+MESH_ID = pl.DeviceIdType.MESH
+
+
+def remote(src, dst, send_sem, recv_sem, sp, tp):
+    return pltpu.make_async_remote_copy(
+        src_ref=src,
+        dst_ref=dst,
+        send_sem=send_sem,
+        recv_sem=recv_sem,
+        device_id=(sp, tp),
+        device_id_type=MESH_ID,
+    )
+
+
+def rows_at(index, count):
+    return pl.ds(pl.multiple_of(index * count, count), count)
+
+
+def greet(n_sp, tp_peers, me_s, me_t):
+    barrier = pltpu.get_barrier_semaphore()
+    for step in range(1, n_sp):
+        pl.semaphore_signal(
+            barrier, inc=1, device_id=((me_s + step) % n_sp, me_t), device_id_type=MESH_ID
+        )
+    for peer in tp_peers:
+        pl.semaphore_signal(barrier, inc=1, device_id=(me_s, peer), device_id_type=MESH_ID)
+    pl.semaphore_wait(barrier, n_sp - 1 + len(tp_peers))
+
+
+def dot_t(lhs, rhs):
+    return lax.dot_general(
+        lhs, rhs, (((1,), (1,)), ((), ())), preferred_element_type=jnp.float32
+    )
+
+
+def attention_kernel(
+    n_sp,
+    n_tp,
+    scale_s,
+    scale_l,
+    pack_ref,
+    qs_ref,
+    ql_ref,
+    proj_ref,
+    out_s_ref,
+    out_l_ref,
+    residual_ref,
+    middle_ref,
+    lat,
+    max_s,
+    sum_s,
+    acc_s,
+    max_l,
+    sum_l,
+    acc_l,
+    part,
+    got,
+    a_send,
+    a_recv,
+    y_send,
+    y_recv,
+    c_send,
+    c_recv,
+    d_send,
+    d_recv,
+    p_send,
+    p_recv,
+):
+    me_s = lax.axis_index("sp")
+    me_t = lax.axis_index("tp")
+    core_t = me_t + 1 - 2 * (me_t % 2)
+    y_t = (me_t + 2) % n_tp
+    far_t = (core_t + 2) % n_tp
+    rows = pack_ref.shape[0]
+    latent_size = proj_ref.shape[0]
+    quarter = rows // n_tp
+    greet(n_sp, (core_t, y_t, far_t), me_s, me_t)
+
+    def gather_copy(step, source, target):
+        return remote(
+            pack_ref.at[rows_at(me_t, quarter), :],
+            lat.at[source, rows_at(me_t, quarter), :],
+            a_send.at[step - 1],
+            a_recv.at[step - 1],
+            target,
+            me_t,
+        )
+
+    def y_copy(step, source, owner):
+        where = lat.at[source, rows_at(owner, quarter), :]
+        return remote(where, where, y_send.at[step - 1], y_recv.at[step - 1], me_s, y_t)
+
+    def c_copy(step, source, owner):
+        where = lat.at[source, rows_at(owner, quarter), :]
+        return remote(where, where, c_send.at[step - 1], c_recv.at[step - 1], me_s, core_t)
+
+    def d_copy(step, source, owner):
+        where = lat.at[source, rows_at(owner, quarter), :]
+        return remote(where, where, d_send.at[step - 1], d_recv.at[step - 1], me_s, core_t)
+
+    def send_on(step, carry):
+        gather_copy(step, me_s, me_s + step).start()
+        return carry
+
+    lax.fori_loop(1, n_sp - me_s, send_on, 0)
+
+    def span(block, first):
+        projected = jnp.dot(
+            block[:, :latent_size], proj_ref[...], preferred_element_type=jnp.float32
+        ).astype(jnp.bfloat16)
+        tile = projected.shape[1] // 4
+        key_s = projected[:, :tile] + block[:, latent_size:]
+        key_l = projected[:, tile : 2 * tile]
+        value_s = projected[:, 2 * tile : 3 * tile]
+        value_l = projected[:, 3 * tile :]
+        query_l = ql_ref[...]
+        score_s = dot_t(qs_ref[...], key_s) * scale_s
+        score_l = (dot_t(query_l[:, :tile], key_l) + dot_t(query_l[:, tile:], key_s)) * scale_l
+        if first:
+            row_pos = lax.broadcasted_iota(jnp.int32, (rows, rows), 0)
+            key_pos = lax.broadcasted_iota(jnp.int32, (rows, rows), 1)
+            allowed = key_pos <= row_pos
+            score_s = jnp.where(allowed, score_s, masked_score)
+            score_l = jnp.where(allowed, score_l, masked_score)
+        for score, value, top, total, acc in (
+            (score_s, value_s, max_s, sum_s, acc_s),
+            (score_l, value_l, max_l, sum_l, acc_l),
+        ):
+            block_top = jnp.max(score, axis=1, keepdims=True)
+            new_top = block_top if first else jnp.maximum(top[...], block_top)
+            weights = jnp.exp(score - new_top)
+            weight_sum = jnp.sum(weights, axis=1, keepdims=True)
+            mixed = jnp.dot(
+                weights.astype(jnp.bfloat16), value, preferred_element_type=jnp.float32
+            )
+            if first:
+                total[...] = weight_sum
+                acc[...] = mixed
+            else:
+                rescale = jnp.exp(top[...] - new_top)
+                total[...] = total[...] * rescale + weight_sum
+                acc[...] = acc[...] * rescale + mixed
+            top[...] = new_top
+
+    span(pack_ref[...], True)
+
+    def pass_on(step, carry):
+        @pl.when(step <= me_s)
+        def _():
+            source = me_s - step
+            gather_copy(step, source, me_s).wait_recv()
+            y_copy(step, source, me_t).start()
+            c_copy(step, source, me_t).start()
+
+        @pl.when((step >= 2) & (step <= me_s + 1))
+        def _():
+            before = step - 1
+            source = me_s - before
+            y_copy(before, source, y_t).wait_recv()
+            d_copy(before, source, y_t).start()
+
+        @pl.when(step >= 3)
+        def _():
+            before = step - 2
+            source = me_s - before
+            c_copy(before, source, core_t).wait_recv()
+            d_copy(before, source, far_t).wait_recv()
+            span(lat[source], False)
+
+        return carry
+
+    lax.fori_loop(1, me_s + 3, pass_on, 0)
+
+    value_s = out_s_ref.shape[0]
+    heads_s = (acc_s[:, :value_s] / sum_s[...]).astype(jnp.bfloat16)
+    heads_l = (acc_l[...] / sum_l[...]).astype(jnp.bfloat16)
+    part[...] = (
+        jnp.dot(heads_s, out_s_ref[...], preferred_element_type=jnp.float32)
+        + jnp.dot(heads_l, out_l_ref[...], preferred_element_type=jnp.float32)
+    ).astype(jnp.bfloat16)
+
+    def part_copy(number, target):
+        return remote(
+            part.at[rows_at(target, quarter), :],
+            got.at[number],
+            p_send.at[number],
+            p_recv.at[number],
+            me_s,
+            target,
+        )
+
+    peers = (far_t, y_t, core_t)
+    for number, peer in enumerate(peers):
+        part_copy(number, peer).start()
+    total = part[rows_at(me_t, quarter), :].astype(jnp.float32)
+    for number, peer in reversed(tuple(enumerate(peers))):
+        part_copy(number, peer).wait_recv()
+        total = total + got[number].astype(jnp.float32)
+    attention = total.astype(jnp.bfloat16).astype(jnp.float32)
+    middle_ref[...] = (residual_ref[...].astype(jnp.float32) + attention).astype(jnp.bfloat16)
+
+    for number, peer in enumerate(peers):
+        part_copy(number, peer).wait_send()
+
+    def drain_gather(step, carry):
+        gather_copy(step, me_s, me_s + step).wait_send()
+        return carry
+
+    lax.fori_loop(1, n_sp - me_s, drain_gather, 0)
+
+    def drain_shared(step, carry):
+        source = me_s - step
+        y_copy(step, source, me_t).wait_send()
+        c_copy(step, source, me_t).wait_send()
+        d_copy(step, source, y_t).wait_send()
+        return carry
+
+    lax.fori_loop(1, me_s + 1, drain_shared, 0)
+
+
+def expert_kernel(
+    n_sp,
+    n_tp,
+    capacity,
+    middle_ref,
+    gain_ref,
+    routing_ref,
+    route_weight_ref,
+    gate_hbm,
+    up_hbm,
+    down_hbm,
+    out_ref,
+    gate_v,
+    up_v,
+    down_v,
+    outgoing,
+    recv,
+    part,
+    pair,
+    y_out,
+    y_in,
+    back_out,
+    back_in,
+    w_sem,
+    a_send,
+    a_recv,
+    y_send,
+    y_recv,
+    c_send,
+    c_recv,
+    d_send,
+    d_recv,
+    p_send,
+    p_recv,
+    z_send,
+    z_recv,
+    b_send,
+    b_recv,
+):
+    me_s = lax.axis_index("sp")
+    me_t = lax.axis_index("tp")
+    core_t = me_t + 1 - 2 * (me_t % 2)
+    y_t = (me_t + 2) % n_tp
+    my_core = me_t % 2
+    my_y = me_t // 2
+    tok_count, width = middle_ref.shape
+    slots = n_sp * capacity
+    loads = (
+        pltpu.make_async_copy(gate_hbm.at[0], gate_v, w_sem.at[0]),
+        pltpu.make_async_copy(up_hbm.at[0], up_v, w_sem.at[1]),
+        pltpu.make_async_copy(down_hbm.at[0], down_v, w_sem.at[2]),
+    )
+    for load in loads:
+        load.start()
+
+    normed = rms_scaled(middle_ref[...], gain_ref[...]).astype(jnp.bfloat16)
+    routing = routing_ref[...]
+    expert_ids = lax.broadcasted_iota(jnp.int32, (tok_count, slots), 1)
+    named = [
+        (routing[:, k : k + 1] == expert_ids).astype(jnp.float32) for k in range(TOPK)
+    ]
+    earlier = (
+        lax.broadcasted_iota(jnp.int32, (tok_count, tok_count), 1)
+        < lax.broadcasted_iota(jnp.int32, (tok_count, tok_count), 0)
+    ).astype(jnp.bfloat16)
+    ahead = jnp.dot(
+        earlier, sum(named).astype(jnp.bfloat16), preferred_element_type=jnp.float32
+    )
+    picks = []
+    for k in range(TOPK):
+        slot = jnp.sum(named[k] * ahead, axis=1, keepdims=True).astype(jnp.int32)
+        picks.append(
+            (routing[:, k : k + 1] * capacity + slot == expert_ids).astype(jnp.float32)
+        )
+    send_table = jnp.transpose(sum(picks)).astype(jnp.bfloat16)
+    outgoing[...] = jnp.dot(
+        send_table, normed, preferred_element_type=jnp.float32
+    ).astype(jnp.bfloat16)
+
+    greet(n_sp, (core_t, y_t), me_s, me_t)
+
+    def block(owner, source):
+        return pl.ds(pl.multiple_of(owner * slots + source * capacity, capacity), capacity)
+
+    def a_copy(step, source, target):
+        return remote(
+            outgoing.at[rows_at(target, capacity), :],
+            recv.at[block(me_t, source), :],
+            a_send.at[step],
+            a_recv.at[step],
+            target,
+            me_t,
+        )
+
+    def shared(send, got, step, owner, target):
+        where = recv.at[block(owner, (me_s + n_sp - step) % n_sp), :]
+        return remote(where, where, send.at[step], got.at[step], me_s, target)
+
+    for step in range(1, n_sp):
+        a_copy(step, me_s, (me_s + step) % n_sp).start()
+    recv[block(me_t, me_s), :] = outgoing[rows_at(me_s, capacity), :]
+    for step in range(n_sp):
+        if step:
+            a_copy(step, (me_s + n_sp - step) % n_sp, me_s).wait_recv()
+        shared(y_send, y_recv, step, me_t, y_t).start()
+        shared(c_send, c_recv, step, me_t, core_t).start()
+        if step:
+            shared(y_send, y_recv, step - 1, y_t, y_t).wait_recv()
+            shared(d_send, d_recv, step - 1, y_t, core_t).start()
+    shared(y_send, y_recv, n_sp - 1, y_t, y_t).wait_recv()
+    shared(d_send, d_recv, n_sp - 1, y_t, core_t).start()
+    for load in loads:
+        load.wait()
+
+    half = 2 * slots
+
+    def hidden_of(y_index):
+        rows_in = recv[rows_at(y_index, half), :]
+        gate_pre = jnp.dot(rows_in, gate_v[...], preferred_element_type=jnp.float32)
+        up_pre = jnp.dot(rows_in, up_v[...], preferred_element_type=jnp.float32)
+        return clamped(gate_pre, up_pre).astype(jnp.bfloat16)
+
+    def down_of(y_index, hidden):
+        part[rows_at(y_index, half), :] = jnp.dot(
+            hidden, down_v[...], preferred_element_type=jnp.float32
+        ).astype(jnp.bfloat16)
+
+    def pair_copy(number, y_index, core_index):
+        return remote(
+            part.at[rows_at(2 * y_index + core_index, slots), :],
+            pair.at[number],
+            p_send.at[number],
+            p_recv.at[number],
+            me_s,
+            core_t,
+        )
+
+    far_core = 1 - my_core
+    far_y = 1 - my_y
+    for step in range(n_sp):
+        shared(d_send, d_recv, step, 2 * far_y + far_core, core_t).wait_recv()
+    down_of(far_y, hidden_of(far_y))
+    pair_copy(0, far_y, far_core).start()
+    for step in range(n_sp):
+        shared(c_send, c_recv, step, core_t, core_t).wait_recv()
+    hidden = hidden_of(my_y)
+    pair_copy(0, far_y, far_core).wait_recv()
+    y_out[...] = (
+        part[rows_at(y_t, slots), :].astype(jnp.float32) + pair[0].astype(jnp.float32)
+    ).astype(jnp.bfloat16)
+
+    def z_copy(step):
+        where = rows_at((me_s + step) % n_sp, capacity)
+        return remote(
+            y_out.at[where, :], y_in.at[where, :], z_send.at[step], z_recv.at[step], me_s, y_t
+        )
+
+    order = tuple(range(1, n_sp)) + (0,)
+    for step in order:
+        z_copy(step).start()
+    down_of(my_y, hidden)
+    pair_copy(1, my_y, far_core).start()
+    pair_copy(1, my_y, far_core).wait_recv()
+
+    def back_copy(step, source, target):
+        return remote(
+            back_out.at[rows_at(target, capacity), :],
+            back_in.at[rows_at(source, capacity), :],
+            b_send.at[step],
+            b_recv.at[step],
+            target,
+            me_t,
+        )
+
+    for step in order:
+        target = (me_s + step) % n_sp
+        z_copy(step).wait_recv()
+        where = rows_at(target, capacity)
+        summed = (
+            part[block(me_t, target), :].astype(jnp.float32)
+            + pair[1, where, :].astype(jnp.float32)
+            + y_in[where, :].astype(jnp.float32)
+        ).astype(jnp.bfloat16)
+        if step:
+            back_out[where, :] = summed
+            back_copy(step, me_s, target).start()
+        else:
+            back_in[where, :] = summed
+    for step in range(1, n_sp):
+        back_copy(step, (me_s + n_sp - step) % n_sp, me_s).wait_recv()
+    returned = back_in[...]
+    mixed = middle_ref[...].astype(jnp.float32)
+    route_weight = route_weight_ref[...]
+    terms = [
+        route_weight[:, k : k + 1]
+        * jnp.dot(picks[k].astype(jnp.bfloat16), returned, preferred_element_type=jnp.float32)
+        for k in range(TOPK)
+    ]
+    out_ref[...] = (mixed + sum(terms)).astype(jnp.bfloat16)
+
+    for step in range(1, n_sp):
+        a_copy(step, me_s, (me_s + step) % n_sp).wait_send()
+        back_copy(step, me_s, (me_s + step) % n_sp).wait_send()
+    for step in range(n_sp):
+        shared(y_send, y_recv, step, me_t, y_t).wait_send()
+        shared(c_send, c_recv, step, me_t, core_t).wait_send()
+        shared(d_send, d_recv, step, y_t, core_t).wait_send()
+        z_copy(step).wait_send()
+    pair_copy(0, far_y, far_core).wait_send()
+    pair_copy(1, my_y, far_core).wait_send()
+
+
+def in_kernels(
+    residual,
+    query_small,
+    query_large,
+    latent,
+    rotary_key,
+    latent_gain,
+    small_keys,
+    small_values,
+    large_keys,
+    large_values,
+    small_output,
+    large_output,
+    ffn_gain,
+    gate_weights,
+    up_weights,
+    down_weights,
+    routing,
+    route_weight,
+):
+    n_sp, n_tp = lax.axis_size("sp"), lax.axis_size("tp")
+    rows, latent_size = latent.shape
+    tok_count, width = residual.shape
+    hidden_units = gate_weights.shape[2]
+    capacity = 2 * TOPK * tok_count // n_sp
+    slots = n_sp * capacity
+    half_rows = 2 * slots
+    tile = NOPE_L
+    first_pos = lax.axis_index("sp") * rows
+    cos_vals, sin_vals = rope_tables(rows, first_pos)
+    small_query = turn_queries(query_small, NOPE_S, cos_vals, sin_vals)[:, 0]
+    large_query = turn_queries(query_large, NOPE_L, cos_vals, sin_vals)[:, 0]
+    after = tile - NOPE_S - ROPE
+    qs = jnp.pad(small_query, ((0, 0), (0, after)))
+    ql = jnp.concatenate(
+        [large_query[:, :NOPE_L], jnp.pad(large_query[:, NOPE_L:], ((0, 0), (NOPE_S, after)))],
+        axis=1,
+    )
+    turned = rotate(rotary_key.astype(jnp.float32), cos_vals, sin_vals).astype(jnp.bfloat16)
+    pack = jnp.concatenate(
+        [
+            rms_scaled(latent, latent_gain).astype(jnp.bfloat16),
+            jnp.pad(turned, ((0, 0), (NOPE_S, after))),
+        ],
+        axis=1,
+    )
+    proj = jnp.concatenate(
+        [
+            jnp.pad(small_keys, ((0, 0), (0, tile - small_keys.shape[1]))),
+            large_keys,
+            jnp.pad(small_values, ((0, 0), (0, tile - small_values.shape[1]))),
+            large_values,
+        ],
+        axis=1,
+    )
+    in_vmem = pl.BlockSpec(memory_space=pltpu.VMEM)
+    in_hbm = pl.BlockSpec(memory_space=pltpu.HBM)
+    dma = pltpu.SemaphoreType.DMA
+    f32, bf16 = jnp.float32, jnp.bfloat16
+    middle = pl.pallas_call(
+        functools.partial(
+            attention_kernel,
+            n_sp,
+            n_tp,
+            (NOPE_S + ROPE) ** (-0.5),
+            (NOPE_L + ROPE) ** (-0.5),
+        ),
+        name="attend",
+        out_shape=jax.ShapeDtypeStruct(residual.shape, bf16),
+        in_specs=[in_vmem] * 7,
+        out_specs=in_vmem,
+        scratch_shapes=[
+            pltpu.VMEM((n_sp,) + pack.shape, bf16),
+            pltpu.VMEM((rows, 1), f32),
+            pltpu.VMEM((rows, 1), f32),
+            pltpu.VMEM((rows, tile), f32),
+            pltpu.VMEM((rows, 1), f32),
+            pltpu.VMEM((rows, 1), f32),
+            pltpu.VMEM((rows, tile), f32),
+            pltpu.VMEM((rows, width), bf16),
+            pltpu.VMEM((n_tp - 1, tok_count, width), bf16),
+        ]
+        + [dma((n_sp - 1,))] * 8
+        + [dma((n_tp - 1,))] * 2,
+        compiler_params=pltpu.CompilerParams(
+            collective_id=0, has_side_effects=True, vmem_limit_bytes=24 * 2**20
+        ),
+    )(pack, qs, ql, proj, small_output, large_output, residual)
+    return pl.pallas_call(
+        functools.partial(expert_kernel, n_sp, n_tp, capacity),
+        name="experts",
+        out_shape=jax.ShapeDtypeStruct(residual.shape, bf16),
+        in_specs=[in_vmem] * 4 + [in_hbm] * 3,
+        out_specs=in_vmem,
+        scratch_shapes=[
+            pltpu.VMEM((width, hidden_units), bf16),
+            pltpu.VMEM((width, hidden_units), bf16),
+            pltpu.VMEM((hidden_units, width), bf16),
+            pltpu.VMEM((slots, width), bf16),
+            pltpu.VMEM((n_tp * slots, width), bf16),
+            pltpu.VMEM((n_tp * slots, width), bf16),
+            pltpu.VMEM((2, slots, width), bf16),
+            pltpu.VMEM((slots, width), bf16),
+            pltpu.VMEM((slots, width), bf16),
+            pltpu.VMEM((slots, width), bf16),
+            pltpu.VMEM((slots, width), bf16),
+            dma((3,)),
+        ]
+        + [dma((n_sp,))] * 8
+        + [dma((2,))] * 2
+        + [dma((n_sp,))] * 4,
+        compiler_params=pltpu.CompilerParams(
+            collective_id=1, has_side_effects=True, vmem_limit_bytes=48 * 2**20
+        ),
+    )(
+        middle,
+        ffn_gain.reshape(1, width),
+        routing,
+        route_weight,
+        gate_weights,
+        up_weights,
+        down_weights,
+    )
+
+
+def choose(*args):
+    residual, latent, gate_weights = args[0], args[3], args[13]
+    n_sp, n_tp = lax.axis_size("sp"), lax.axis_size("tp")
+    tok_count = residual.shape[0]
+    capacity = 2 * TOPK * tok_count // (n_sp * gate_weights.shape[0])
+    fits = (
+        n_tp == 4
+        and gate_weights.shape[0] == 1
+        and capacity > 0
+        and capacity % 16 == 0
+        and n_sp * capacity % 128 == 0
+        and tok_count % 16 == 0
+        and args[6].shape[1] == NOPE_S
+        and args[8].shape[1] == NOPE_L
+    )
+    return in_kernels(*args) if fits else on_device(*args)
+
+
 def solution(mesh):
     return jax.shard_map(
-        on_device,
+        choose,
         mesh=mesh,
         in_specs=(
             P(("sp", "tp"), None),

time: 207 us -> 89.9 us (0.43)
  waiting for transfers between devices: 88.5 us -> 0 us
  Pallas kernels: 0 us -> 77.7 us
  blocking collectives: 67.6 us -> 0 us
  matrix products: 26 us -> 0 us
  between operations: 13.2 us -> 0.2 us
  other arithmetic: 8.79 us -> 4.86 us
  local copies, waits for them, and re-layouts: 1.97 us -> 5.49 us
    pallas_call x0 -> x2, Pallas kernels: none -> 77.7 us  [the longest x1 62.2 us: in_kernels(): pl.pallas_call(functools.partial(expert_kernel, n_sp, n_tp, capacity), na...]
    reduce_scatter x2 -> x0, waiting for transfers between devices: 51 us -> none  [the longest x1 31.3 us: on_device(): lax.psum_scatter(partials.astype(jnp.bfloat16), 'tp', scatter_dimension=0...]
    all_to_all x2 -> x0, blocking collectives: 39.6 us -> none  [the longest x1 19.9 us: on_device(): lax.all_to_all(combined, 'sp', split_axis=0, concat_axis=0, tiled=True)]
    all_gather x2 -> x0, waiting for transfers between devices: 36.7 us -> none  [the longest x1 20.8 us: on_device(): lax.all_gather(lax.all_to_all(outgoing, 'sp', split_axis=0, concat_axis=0...]
    all_gather x1 -> x0, blocking collectives: 28 us -> none  [on_device(): lax.all_gather(rotary_key, 'sp', axis=0, tiled=True)]
    dot_general x12 -> x0, matrix products: 26 us -> none  [the longest x1 6.02 us: on_device(): jnp.einsum('secf,efd->secd', hidden, down_weights, preferred_element_type...]
    unnamed x13 -> x25, local copies, waits for them, and re-layouts: 0.12 us -> 5.34 us
    reduce_sum x3 -> x0, other arithmetic: 2.07 us -> none  [the longest x1 1.81 us: update(): weight_sum = jnp.sum(weights, axis=2)]
  transfers between devices with their start and end apart: 4 -> 0, of which waited for: 4 -> 0; matrix products, arithmetic and copies ran while one was open for 1% -> 0% of each run, Pallas kernels for 0% -> 0%
where the time goes in v1:
time: 89.9 us; the launch traced here: 88.3 us
  Pallas kernels  77.7 us (86%)
  local copies, waits for them, and re-layouts  5.49 us (6%)
  other arithmetic  4.86 us (5%)
    pallas_call x1, Pallas kernels, in_kernels(): pl.pallas_call(functools.partial(expert_kernel, n_sp, n_tp, capacity), na...  62.2 us
    pallas_call x1, Pallas kernels, in_kernels(): pl.pallas_call(functools.partial(attention_kernel, n_sp, n_tp, (NOPE_S +...  15.5 us
    unnamed x25, local copies, waits for them, and re-layouts  5.34 us

profile of v1, /device:TPU:0, one launch (start us, length us, event | category | flops | bytes accessed | tf_op | source)
XLA Modules:
  0.0 88.3 jit_solution(1003466973103823836)
XLA Ops:
  0.0 0.0 copy-start.6
  0.0 0.0 copy-start.4
  0.0 0.0 copy-start.3
  0.0 0.0 copy-start.2
  0.0 1.0 %copy.36 = bf16[128,160]{1,0:T(8,128)(2,1)S(1)} copy(bf16[128,160]{0,1:T(8,128)(2,1)} %param.20) | data formatting | bytes 81920 | tf_op args[2]
  1.0 0.8 copy.34
  1.8 0.1 slice_convert_fusion
  1.9 0.3 fusion.25
  2.3 0.1 maximum_bitcast_fusion
  2.4 0.1 fusion.28.ql_ref
  2.5 0.1 maximum_bitcast_fusion.1
  2.6 0.0 copy-start.7
  2.6 0.0 copy-start.8
  2.6 0.0 copy-start
  2.6 0.0 copy-start.5
  2.7 0.8 convert_element_type.51
  3.5 0.1 fusion.34
  3.6 0.1 copy.33
  3.8 1.0 %fusion.7 = f32[128]{0:T(128)S(1)} fusion(bf16[128,512]{1,0:T(8,128)(2,1)} %param.21), kind=kLoop, calls=%fused_computation.13 | loop fusion | flops 196480 | bytes 131584 | tf_op jit(solution)/shard_map/reduce_sum | solution.py:44
  4.8 1.0 %fusion.9 = bf16[128,512]{1,0:T(8,128)(2,1)S(1)} fusion(bf16[128,512]{1,0:T(8,128)(2,1)} %param.21, f32[512]{0:T(512)} %param.23, f32[128]{0:T(128)S(1)} %add_rsqrt_fusion), kind=kLoop, calls=%fused_computation.15 | loop fusion | flops 262144 | bytes 264704 | tf_op jit(solution)/shard_map/convert_element_type | solution.py:703
  5.8 0.1 fusion.10.pack_ref
  5.9 0.0 copy-done.6
  5.9 0.1 copy.37
  6.0 1.0 %copy.38 = bf16[512,64]{1,0:T(8,128)(2,1)S(1)} copy(bf16[512,64]{0,1:T(8,128)(2,1)} %param.25) | data formatting | bytes 131072 | tf_op args[7]
  7.0 1.1 %fusion.4.proj_ref = bf16[512,512]{1,0:T(8,128)(2,1)S(1)} fusion(bf16[512,64]{1,0:T(8,128)(2,1)S(1)} %copy.38, bf16[512,64]{1,0:T(8,128)(2,1)S(1)} %copy.37, bf16[512,128]{1,0:T(8,128)(2,1)} %param.27, bf16[512,128]{1,0:T(8,128)(2,1)} %param.26), kind=kLoop, calls=%fused_computation.7 | loop fusion | flops 3670016 | bytes 917504 | tf_op jit(solution)/shard_map/concatenate | solution.py:708
  8.1 0.0 copy-done.4
  8.1 0.0 copy-done.3
  8.1 0.0 copy-done.2
  8.1 15.5 %attend.1.middle_ref = bf16[32,2048]{1,0:T(8,128)(2,1)S(1)} custom-call(bf16[128,640]{1,0:T(8,128)(2,1)S(1)} %fusion.10.pack_ref, bf16[128,128]{1,0:T(8,128)(2,1)S(1)} %pad.19.qs_ref, bf16[128,256]{1,0:T(8,128)(2,1)S(1)} %fusion.28.ql_ref, bf16[512,512]{1,0:T(8,128)(2,1)S(1)} %fusion.4.proj_ref, bf16[64,2048]{1,0:T(8,128)(2,1)S(1)} %copy-done.3, ...), custom_call_target="tpu_custom_call" | custom-call | tf_op jit(solution)/shard_map/attend/pallas_call | solution.py:721
  23.6 0.0 copy-done.7
  23.6 0.1 copy.39.routing_ref
  23.7 0.0 copy-done.8
  23.7 0.1 copy.40.route_weight_ref
  23.8 0.0 copy-done
  23.8 0.0 copy-done.5
  23.8 0.0 copy-start.1
  23.8 1.6 %copy-done.1 = bf16[1,2048,512]{2,1,0:T(8,128)(2,1)S(1)} copy-done((bf16[1,2048,512]{2,1,0:T(8,128)(2,1)S(1)}, bf16[1,2048,512]{2,1,0:T(8,128)(2,1)}, u32[]{:S(2)}) %copy-start.1) | copy-done | bytes 2097176
  25.4 62.2 %experts.1 = bf16[32,2048]{1,0:T(8,128)(2,1)S(1)} custom-call(bf16[32,2048]{1,0:T(8,128)(2,1)S(1)} %attend.1.middle_ref, f32[1,2048]{1,0:T(1,128)S(1)} %bitcast.8, s32[32,2]{1,0:T(8,128)S(1)} %copy.39.routing_ref, f32[32,2]{1,0:T(8,128)S(1)} %copy.40.route_weight_ref, bf16[1,2048,512]{2,1,0:T(8,128)(2,1)S(1)} %copy-done, ...), custom_call_target="tpu_custom_call" | custom-call | tf_op jit(solution)/shard_map/experts/pallas_call | solution.py:750
  87.6 0.7 copy.42
  (8 shorter events, 0.0 us)
Async XLA Ops:
  0.0 5.9 %copy-start.6 = (bf16[512,64]{0,1:T(8,128)(2,1)S(1)}, bf16[512,64]{0,1:T(8,128)(2,1)}, u32[]{:S(2)}) copy-start(bf16[512,64]{0,1:T(8,128)(2,1)} %param.24) | copy-start | bytes 196612
  0.0 8.1 %copy-start.4 = (bf16[32,2048]{1,0:T(8,128)(2,1)S(1)}, bf16[32,2048]{1,0:T(8,128)(2,1)}, u32[]{:S(2)}) copy-start(bf16[32,2048]{1,0:T(8,128)(2,1)} %residual_ref.1) | copy-start | bytes 393220
  0.0 8.1 %copy-start.3 = (bf16[64,2048]{1,0:T(8,128)(2,1)S(1)}, bf16[64,2048]{1,0:T(8,128)(2,1)}, u32[]{:S(2)}) copy-start(bf16[64,2048]{1,0:T(8,128)(2,1)} %out_s_ref.1) | copy-start | bytes 786436
  0.0 8.1 %copy-start.2 = (bf16[128,2048]{1,0:T(8,128)(2,1)S(1)}, bf16[128,2048]{1,0:T(8,128)(2,1)}, u32[]{:S(2)}) copy-start(bf16[128,2048]{1,0:T(8,128)(2,1)} %out_l_ref.1) | copy-start | bytes 1572868
  2.6 21.0 %copy-start.7 = (s32[32,2]{0,1:T(2,128)S(1)}, s32[32,2]{0,1:T(2,128)}, u32[]{:S(2)}) copy-start(s32[32,2]{0,1:T(2,128)} %param.34) | copy-start | bytes 772
  2.6 21.1 %copy-start.8 = (f32[32,2]{0,1:T(2,128)S(1)}, f32[32,2]{0,1:T(2,128)}, u32[]{:S(2)}) copy-start(f32[32,2]{0,1:T(2,128)} %param.35) | copy-start | bytes 772
  2.6 21.1 %copy-start = (bf16[1,2048,512]{2,1,0:T(8,128)(2,1)S(1)}, bf16[1,2048,512]{2,1,0:T(8,128)(2,1)}, u32[]{:S(2)}) copy-start(bf16[1,2048,512]{2,1,0:T(8,128)(2,1)} %gate_hbm.1) | copy-start | bytes 6291460
  2.6 21.1 %copy-start.5 = (f32[2048]{0:T(1024)S(1)}, f32[2048]{0:T(1024)}, u32[]{:S(2)}) copy-start(f32[2048]{0:T(1024)} %param.30) | copy-start | bytes 24580
  23.8 1.6 %copy-start.1 = (bf16[1,2048,512]{2,1,0:T(8,128)(2,1)S(1)}, bf16[1,2048,512]{2,1,0:T(8,128)(2,1)}, u32[]{:S(2)}) copy-start(bf16[1,2048,512]{2,1,0:T(8,128)(2,1)} %up_hbm.1) | copy-start | bytes 6291460

commit v2 on v1

--- a/solution.py
+++ b/solution.py
@@ -2,6 +2,7 @@
 
 import jax
 import jax.numpy as jnp
+import numpy as np
 from jax import lax
 from jax.experimental import pallas as pl
 from jax.experimental.pallas import tpu as pltpu
@@ -253,7 +254,7 @@
         )
     for peer in tp_peers:
         pl.semaphore_signal(barrier, inc=1, device_id=(me_s, peer), device_id_type=MESH_ID)
-    pl.semaphore_wait(barrier, n_sp - 1 + len(tp_peers))
+    return lambda: pl.semaphore_wait(barrier, n_sp - 1 + len(tp_peers))
 
 
 def dot_t(lhs, rhs):
@@ -262,196 +263,31 @@
     )
 
 
-def attention_kernel(
+def turned_rows(front, back, cos_vals, sin_vals):
+    front, back = front.astype(jnp.float32), back.astype(jnp.float32)
+    return jnp.concatenate(
+        [front * cos_vals - back * sin_vals, back * cos_vals + front * sin_vals], axis=0
+    )
+
+
+def layer_kernel(
     n_sp,
     n_tp,
-    scale_s,
-    scale_l,
-    pack_ref,
+    capacity,
+    latent_ref,
+    rotary_ref,
+    latent_gain_ref,
+    cos_ref,
+    sin_ref,
     qs_ref,
     ql_ref,
-    proj_ref,
+    keys_s_ref,
+    values_s_ref,
+    keys_l_ref,
+    values_l_ref,
     out_s_ref,
     out_l_ref,
     residual_ref,
-    middle_ref,
-    lat,
-    max_s,
-    sum_s,
-    acc_s,
-    max_l,
-    sum_l,
-    acc_l,
-    part,
-    got,
-    a_send,
-    a_recv,
-    y_send,
-    y_recv,
-    c_send,
-    c_recv,
-    d_send,
-    d_recv,
-    p_send,
-    p_recv,
-):
-    me_s = lax.axis_index("sp")
-    me_t = lax.axis_index("tp")
-    core_t = me_t + 1 - 2 * (me_t % 2)
-    y_t = (me_t + 2) % n_tp
-    far_t = (core_t + 2) % n_tp
-    rows = pack_ref.shape[0]
-    latent_size = proj_ref.shape[0]
-    quarter = rows // n_tp
-    greet(n_sp, (core_t, y_t, far_t), me_s, me_t)
-
-    def gather_copy(step, source, target):
-        return remote(
-            pack_ref.at[rows_at(me_t, quarter), :],
-            lat.at[source, rows_at(me_t, quarter), :],
-            a_send.at[step - 1],
-            a_recv.at[step - 1],
-            target,
-            me_t,
-        )
-
-    def y_copy(step, source, owner):
-        where = lat.at[source, rows_at(owner, quarter), :]
-        return remote(where, where, y_send.at[step - 1], y_recv.at[step - 1], me_s, y_t)
-
-    def c_copy(step, source, owner):
-        where = lat.at[source, rows_at(owner, quarter), :]
-        return remote(where, where, c_send.at[step - 1], c_recv.at[step - 1], me_s, core_t)
-
-    def d_copy(step, source, owner):
-        where = lat.at[source, rows_at(owner, quarter), :]
-        return remote(where, where, d_send.at[step - 1], d_recv.at[step - 1], me_s, core_t)
-
-    def send_on(step, carry):
-        gather_copy(step, me_s, me_s + step).start()
-        return carry
-
-    lax.fori_loop(1, n_sp - me_s, send_on, 0)
-
-    def span(block, first):
-        projected = jnp.dot(
-            block[:, :latent_size], proj_ref[...], preferred_element_type=jnp.float32
-        ).astype(jnp.bfloat16)
-        tile = projected.shape[1] // 4
-        key_s = projected[:, :tile] + block[:, latent_size:]
-        key_l = projected[:, tile : 2 * tile]
-        value_s = projected[:, 2 * tile : 3 * tile]
-        value_l = projected[:, 3 * tile :]
-        query_l = ql_ref[...]
-        score_s = dot_t(qs_ref[...], key_s) * scale_s
-        score_l = (dot_t(query_l[:, :tile], key_l) + dot_t(query_l[:, tile:], key_s)) * scale_l
-        if first:
-            row_pos = lax.broadcasted_iota(jnp.int32, (rows, rows), 0)
-            key_pos = lax.broadcasted_iota(jnp.int32, (rows, rows), 1)
-            allowed = key_pos <= row_pos
-            score_s = jnp.where(allowed, score_s, masked_score)
-            score_l = jnp.where(allowed, score_l, masked_score)
-        for score, value, top, total, acc in (
-            (score_s, value_s, max_s, sum_s, acc_s),
-            (score_l, value_l, max_l, sum_l, acc_l),
-        ):
-            block_top = jnp.max(score, axis=1, keepdims=True)
-            new_top = block_top if first else jnp.maximum(top[...], block_top)
-            weights = jnp.exp(score - new_top)
-            weight_sum = jnp.sum(weights, axis=1, keepdims=True)
-            mixed = jnp.dot(
-                weights.astype(jnp.bfloat16), value, preferred_element_type=jnp.float32
-            )
-            if first:
-                total[...] = weight_sum
-                acc[...] = mixed
-            else:
-                rescale = jnp.exp(top[...] - new_top)
-                total[...] = total[...] * rescale + weight_sum
-                acc[...] = acc[...] * rescale + mixed
-            top[...] = new_top
-
-    span(pack_ref[...], True)
-
-    def pass_on(step, carry):
-        @pl.when(step <= me_s)
-        def _():
-            source = me_s - step
-            gather_copy(step, source, me_s).wait_recv()
-            y_copy(step, source, me_t).start()
-            c_copy(step, source, me_t).start()
-
-        @pl.when((step >= 2) & (step <= me_s + 1))
-        def _():
-            before = step - 1
-            source = me_s - before
-            y_copy(before, source, y_t).wait_recv()
-            d_copy(before, source, y_t).start()
-
-        @pl.when(step >= 3)
-        def _():
-            before = step - 2
-            source = me_s - before
-            c_copy(before, source, core_t).wait_recv()
-            d_copy(before, source, far_t).wait_recv()
-            span(lat[source], False)
-
-        return carry
-
-    lax.fori_loop(1, me_s + 3, pass_on, 0)
-
-    value_s = out_s_ref.shape[0]
-    heads_s = (acc_s[:, :value_s] / sum_s[...]).astype(jnp.bfloat16)
-    heads_l = (acc_l[...] / sum_l[...]).astype(jnp.bfloat16)
-    part[...] = (
-        jnp.dot(heads_s, out_s_ref[...], preferred_element_type=jnp.float32)
-        + jnp.dot(heads_l, out_l_ref[...], preferred_element_type=jnp.float32)
-    ).astype(jnp.bfloat16)
-
-    def part_copy(number, target):
-        return remote(
-            part.at[rows_at(target, quarter), :],
-            got.at[number],
-            p_send.at[number],
-            p_recv.at[number],
-            me_s,
-            target,
-        )
-
-    peers = (far_t, y_t, core_t)
-    for number, peer in enumerate(peers):
-        part_copy(number, peer).start()
-    total = part[rows_at(me_t, quarter), :].astype(jnp.float32)
-    for number, peer in reversed(tuple(enumerate(peers))):
-        part_copy(number, peer).wait_recv()
-        total = total + got[number].astype(jnp.float32)
-    attention = total.astype(jnp.bfloat16).astype(jnp.float32)
-    middle_ref[...] = (residual_ref[...].astype(jnp.float32) + attention).astype(jnp.bfloat16)
-
-    for number, peer in enumerate(peers):
-        part_copy(number, peer).wait_send()
-
-    def drain_gather(step, carry):
-        gather_copy(step, me_s, me_s + step).wait_send()
-        return carry
-
-    lax.fori_loop(1, n_sp - me_s, drain_gather, 0)
-
-    def drain_shared(step, carry):
-        source = me_s - step
-        y_copy(step, source, me_t).wait_send()
-        c_copy(step, source, me_t).wait_send()
-        d_copy(step, source, y_t).wait_send()
-        return carry
-
-    lax.fori_loop(1, me_s + 1, drain_shared, 0)
-
-
-def expert_kernel(
-    n_sp,
-    n_tp,
-    capacity,
-    middle_ref,
     gain_ref,
     routing_ref,
     route_weight_ref,
@@ -459,6 +295,15 @@
     up_hbm,
     down_hbm,
     out_ref,
+    pack_ref,
+    lat,
+    proj_ref,
+    queries,
+    scores,
+    values,
+    part_a,
+    got,
+    middle_ref,
     gate_v,
     up_v,
     down_v,
@@ -470,6 +315,16 @@
     y_in,
     back_out,
     back_in,
+    ga_send,
+    ga_recv,
+    gy_send,
+    gy_recv,
+    gc_send,
+    gc_recv,
+    gd_send,
+    gd_recv,
+    o_send,
+    o_recv,
     w_sem,
     a_send,
     a_recv,
@@ -490,43 +345,213 @@
     me_t = lax.axis_index("tp")
     core_t = me_t + 1 - 2 * (me_t % 2)
     y_t = (me_t + 2) % n_tp
+    far_t = (core_t + 2) % n_tp
+    rows, latent_size = latent_ref.shape
+    tile = keys_l_ref.shape[1]
+    quarter = rows // n_tp
+    everyone = greet(n_sp, (core_t, y_t, far_t), me_s, me_t)
+    loads = (
+        pltpu.make_async_copy(gate_hbm.at[0], gate_v, w_sem.at[0]),
+        pltpu.make_async_copy(up_hbm.at[0], up_v, w_sem.at[1]),
+        pltpu.make_async_copy(down_hbm.at[0], down_v, w_sem.at[2]),
+    )
+    for load in loads:
+        load.start()
+
+    half_rope = ROPE // 2
+    places = rows_at(me_s, rows)
+    cos_vals, sin_vals = cos_ref[:, places], sin_ref[:, places]
+
+    def rope_tile(ref, first):
+        return turned_rows(
+            ref[first : first + half_rope, :],
+            ref[first + half_rope : first + ROPE, :],
+            cos_vals,
+            sin_vals,
+        )
+
+    def zero_rows(count, size):
+        return jnp.zeros((count, size), jnp.float32)
+
+    after = tile - NOPE_S - ROPE
+    rotary_tile = jnp.concatenate(
+        [zero_rows(NOPE_S, rows), rope_tile(rotary_ref, 0), zero_rows(after, rows)], axis=0
+    )
+    pack_ref[:, :latent_size] = rms_scaled(latent_ref[...], latent_gain_ref[...]).astype(
+        jnp.bfloat16
+    )
+    pack_ref[:, latent_size:] = jnp.transpose(rotary_tile).astype(jnp.bfloat16)
+    everyone()
+
+    def gather_copy(step, source, target):
+        return remote(
+            pack_ref.at[rows_at(me_t, quarter), :],
+            lat.at[source, rows_at(me_t, quarter), :],
+            ga_send.at[step - 1],
+            ga_recv.at[step - 1],
+            target,
+            me_t,
+        )
+
+    def share_copy(send, got_sem, step, source, owner, target):
+        where = lat.at[source, rows_at(owner, quarter), :]
+        return remote(where, where, send.at[step - 1], got_sem.at[step - 1], me_s, target)
+
+    def y_copy(step, source, owner):
+        return share_copy(gy_send, gy_recv, step, source, owner, y_t)
+
+    def c_copy(step, source, owner):
+        return share_copy(gc_send, gc_recv, step, source, owner, core_t)
+
+    def d_copy(step, source, owner):
+        return share_copy(gd_send, gd_recv, step, source, owner, core_t)
+
+    def send_on(step, carry):
+        gather_copy(step, me_s, me_s + step).start()
+        return carry
+
+    lax.fori_loop(1, n_sp - me_s, send_on, 0)
+
+    query_s = jnp.concatenate(
+        [
+            qs_ref[:NOPE_S, :].astype(jnp.float32),
+            rope_tile(qs_ref, NOPE_S),
+            zero_rows(after, rows),
+        ],
+        axis=0,
+    )
+    query_l = jnp.concatenate(
+        [zero_rows(NOPE_S, rows), rope_tile(ql_ref, NOPE_L), zero_rows(after, rows)], axis=0
+    )
+    queries[0] = jnp.transpose(query_s).astype(jnp.bfloat16)
+    queries[1] = jnp.transpose(ql_ref[:NOPE_L, :].astype(jnp.float32)).astype(jnp.bfloat16)
+    queries[2] = jnp.transpose(query_l).astype(jnp.bfloat16)
+    for number, ref in ((0, keys_s_ref), (2, values_s_ref)):
+        wide = jnp.concatenate(
+            [ref[...].astype(jnp.float32), zero_rows(tile - ref.shape[0], latent_size)], axis=0
+        )
+        proj_ref[:, number * tile : (number + 1) * tile] = jnp.transpose(wide).astype(
+            jnp.bfloat16
+        )
+    proj_ref[:, tile : 2 * tile] = keys_l_ref[...]
+    proj_ref[:, 3 * tile :] = values_l_ref[...]
+    scores[...] = jnp.full(scores.shape, masked_score, jnp.float32)
+    values[...] = jnp.zeros(values.shape, jnp.bfloat16)
+    scale_s = (NOPE_S + ROPE) ** (-0.5)
+    scale_l = (NOPE_L + ROPE) ** (-0.5)
+
+    def span(block_rows, source, first):
+        projected = jnp.dot(
+            block_rows[:, :latent_size], proj_ref[...], preferred_element_type=jnp.float32
+        ).astype(jnp.bfloat16)
+        key_s = projected[:, :tile] + block_rows[:, latent_size:]
+        key_l = projected[:, tile : 2 * tile]
+        where = rows_at(source, rows)
+        values[where, :] = projected[:, 2 * tile :]
+        score_s = dot_t(queries[0], key_s) * scale_s
+        score_l = (dot_t(queries[1], key_l) + dot_t(queries[2], key_s)) * scale_l
+        if first:
+            row_pos = lax.broadcasted_iota(jnp.int32, (rows, rows), 0)
+            key_pos = lax.broadcasted_iota(jnp.int32, (rows, rows), 1)
+            allowed = key_pos <= row_pos
+            score_s = jnp.where(allowed, score_s, masked_score)
+            score_l = jnp.where(allowed, score_l, masked_score)
+        scores[0, :, where] = score_s
+        scores[1, :, where] = score_l
+
+    span(pack_ref[...], me_s, True)
+
+    def pass_on(step, carry):
+        @pl.when(step <= me_s)
+        def _():
+            source = me_s - step
+            gather_copy(step, source, me_s).wait_recv()
+            y_copy(step, source, me_t).start()
+            c_copy(step, source, me_t).start()
+
+        @pl.when((step >= 2) & (step <= me_s + 1))
+        def _():
+            before = step - 1
+            source = me_s - before
+            y_copy(before, source, y_t).wait_recv()
+            d_copy(before, source, y_t).start()
+
+        @pl.when(step >= 3)
+        def _():
+            before = step - 2
+            source = me_s - before
+            c_copy(before, source, core_t).wait_recv()
+            d_copy(before, source, far_t).wait_recv()
+            span(lat[source], source, False)
+
+        return carry
+
+    lax.fori_loop(1, me_s + 3, pass_on, 0)
+
+    def mixed_head(number):
+        score = scores[number]
+        top = jnp.max(score, axis=1, keepdims=True)
+        weights = jnp.exp(score - top)
+        total = jnp.sum(weights, axis=1, keepdims=True)
+        summed = jnp.dot(
+            weights.astype(jnp.bfloat16),
+            values[:, number * tile : (number + 1) * tile],
+            preferred_element_type=jnp.float32,
+        )
+        return (summed / total).astype(jnp.bfloat16)
+
+    heads_s = mixed_head(0)[:, : out_s_ref.shape[0]]
+    heads_l = mixed_head(1)
+    part_a[...] = (
+        jnp.dot(heads_s, out_s_ref[...], preferred_element_type=jnp.float32)
+        + jnp.dot(heads_l, out_l_ref[...], preferred_element_type=jnp.float32)
+    ).astype(jnp.bfloat16)
+
+    def part_copy(number, target):
+        return remote(
+            part_a.at[rows_at(target, quarter), :],
+            got.at[number],
+            o_send.at[number],
+            o_recv.at[number],
+            me_s,
+            target,
+        )
+
+    peers = (far_t, y_t, core_t)
+    for number, peer in enumerate(peers):
+        part_copy(number, peer).start()
+    total = part_a[rows_at(me_t, quarter), :].astype(jnp.float32)
+    for number, peer in reversed(tuple(enumerate(peers))):
+        part_copy(number, peer).wait_recv()
+        total = total + got[number].astype(jnp.float32)
+    attention = total.astype(jnp.bfloat16).astype(jnp.float32)
+    middle_ref[...] = (residual_ref[...].astype(jnp.float32) + attention).astype(jnp.bfloat16)
+
     my_core = me_t % 2
     my_y = me_t // 2
     tok_count, width = middle_ref.shape
     slots = n_sp * capacity
-    loads = (
-        pltpu.make_async_copy(gate_hbm.at[0], gate_v, w_sem.at[0]),
-        pltpu.make_async_copy(up_hbm.at[0], up_v, w_sem.at[1]),
-        pltpu.make_async_copy(down_hbm.at[0], down_v, w_sem.at[2]),
-    )
-    for load in loads:
-        load.start()
-
     normed = rms_scaled(middle_ref[...], gain_ref[...]).astype(jnp.bfloat16)
     routing = routing_ref[...]
-    expert_ids = lax.broadcasted_iota(jnp.int32, (tok_count, slots), 1)
-    named = [
-        (routing[:, k : k + 1] == expert_ids).astype(jnp.float32) for k in range(TOPK)
-    ]
+    expert_ids = lax.broadcasted_iota(jnp.int32, (slots, tok_count), 0)
+    named = [(routing[k : k + 1, :] == expert_ids).astype(jnp.float32) for k in range(TOPK)]
     earlier = (
-        lax.broadcasted_iota(jnp.int32, (tok_count, tok_count), 1)
-        < lax.broadcasted_iota(jnp.int32, (tok_count, tok_count), 0)
+        lax.broadcasted_iota(jnp.int32, (tok_count, tok_count), 0)
+        < lax.broadcasted_iota(jnp.int32, (tok_count, tok_count), 1)
     ).astype(jnp.bfloat16)
     ahead = jnp.dot(
-        earlier, sum(named).astype(jnp.bfloat16), preferred_element_type=jnp.float32
+        sum(named).astype(jnp.bfloat16), earlier, preferred_element_type=jnp.float32
     )
     picks = []
     for k in range(TOPK):
-        slot = jnp.sum(named[k] * ahead, axis=1, keepdims=True).astype(jnp.int32)
+        slot = jnp.sum(named[k] * ahead, axis=0, keepdims=True).astype(jnp.int32)
         picks.append(
-            (routing[:, k : k + 1] * capacity + slot == expert_ids).astype(jnp.float32)
-        )
-    send_table = jnp.transpose(sum(picks)).astype(jnp.bfloat16)
+            (routing[k : k + 1, :] * capacity + slot == expert_ids).astype(jnp.float32)
+        )
+    send_table = sum(picks).astype(jnp.bfloat16)
     outgoing[...] = jnp.dot(
         send_table, normed, preferred_element_type=jnp.float32
     ).astype(jnp.bfloat16)
-
-    greet(n_sp, (core_t, y_t), me_s, me_t)
 
     def block(owner, source):
         return pl.ds(pl.multiple_of(owner * slots + source * capacity, capacity), capacity)
@@ -640,11 +665,17 @@
     returned = back_in[...]
     mixed = middle_ref[...].astype(jnp.float32)
     route_weight = route_weight_ref[...]
-    terms = [
-        route_weight[:, k : k + 1]
-        * jnp.dot(picks[k].astype(jnp.bfloat16), returned, preferred_element_type=jnp.float32)
-        for k in range(TOPK)
-    ]
+    terms = []
+    for k in range(TOPK):
+        weighted = jnp.transpose(picks[k] * route_weight[k : k + 1, :])
+        terms.append(
+            jnp.sum(weighted, axis=1, keepdims=True)
+            * jnp.dot(
+                jnp.transpose(picks[k]).astype(jnp.bfloat16),
+                returned,
+                preferred_element_type=jnp.float32,
+            )
+        )
     out_ref[...] = (mixed + sum(terms)).astype(jnp.bfloat16)
 
     for step in range(1, n_sp):
@@ -657,6 +688,24 @@
         z_copy(step).wait_send()
     pair_copy(0, far_y, far_core).wait_send()
     pair_copy(1, my_y, far_core).wait_send()
+
+    for number, peer in enumerate(peers):
+        part_copy(number, peer).wait_send()
+
+    def drain_gather(step, carry):
+        gather_copy(step, me_s, me_s + step).wait_send()
+        return carry
+
+    lax.fori_loop(1, n_sp - me_s, drain_gather, 0)
+
+    def drain_shared(step, carry):
+        source = me_s - step
+        y_copy(step, source, me_t).wait_send()
+        c_copy(step, source, me_t).wait_send()
+        d_copy(step, source, y_t).wait_send()
+        return carry
+
+    lax.fori_loop(1, me_s + 1, drain_shared, 0)
 
 
 def in_kernels(
@@ -685,75 +734,34 @@
     hidden_units = gate_weights.shape[2]
     capacity = 2 * TOPK * tok_count // n_sp
     slots = n_sp * capacity
-    half_rows = 2 * slots
     tile = NOPE_L
-    first_pos = lax.axis_index("sp") * rows
-    cos_vals, sin_vals = rope_tables(rows, first_pos)
-    small_query = turn_queries(query_small, NOPE_S, cos_vals, sin_vals)[:, 0]
-    large_query = turn_queries(query_large, NOPE_L, cos_vals, sin_vals)[:, 0]
-    after = tile - NOPE_S - ROPE
-    qs = jnp.pad(small_query, ((0, 0), (0, after)))
-    ql = jnp.concatenate(
-        [large_query[:, :NOPE_L], jnp.pad(large_query[:, NOPE_L:], ((0, 0), (NOPE_S, after)))],
-        axis=1,
-    )
-    turned = rotate(rotary_key.astype(jnp.float32), cos_vals, sin_vals).astype(jnp.bfloat16)
-    pack = jnp.concatenate(
-        [
-            rms_scaled(latent, latent_gain).astype(jnp.bfloat16),
-            jnp.pad(turned, ((0, 0), (NOPE_S, after))),
-        ],
-        axis=1,
-    )
-    proj = jnp.concatenate(
-        [
-            jnp.pad(small_keys, ((0, 0), (0, tile - small_keys.shape[1]))),
-            large_keys,
-            jnp.pad(small_values, ((0, 0), (0, tile - small_values.shape[1]))),
-            large_values,
-        ],
-        axis=1,
-    )
+    frequencies = np.float32(rope_base) ** (
+        -np.arange(ROPE // 2, dtype=np.float32) * np.float32(2.0 / ROPE)
+    )
+    places = np.arange(n_sp * rows, dtype=np.float32)
+    angles = (frequencies[:, None] * places[None, :]).astype(np.float32)
+    cos_table = jnp.asarray(np.cos(angles), jnp.float32)
+    sin_table = jnp.asarray(np.sin(angles), jnp.float32)
     in_vmem = pl.BlockSpec(memory_space=pltpu.VMEM)
     in_hbm = pl.BlockSpec(memory_space=pltpu.HBM)
     dma = pltpu.SemaphoreType.DMA
     f32, bf16 = jnp.float32, jnp.bfloat16
-    middle = pl.pallas_call(
-        functools.partial(
-            attention_kernel,
-            n_sp,
-            n_tp,
-            (NOPE_S + ROPE) ** (-0.5),
-            (NOPE_L + ROPE) ** (-0.5),
-        ),
-        name="attend",
+    return pl.pallas_call(
+        functools.partial(layer_kernel, n_sp, n_tp, capacity),
+        name="layer",
         out_shape=jax.ShapeDtypeStruct(residual.shape, bf16),
-        in_specs=[in_vmem] * 7,
+        in_specs=[in_vmem] * 17 + [in_hbm] * 3,
         out_specs=in_vmem,
         scratch_shapes=[
-            pltpu.VMEM((n_sp,) + pack.shape, bf16),
-            pltpu.VMEM((rows, 1), f32),
-            pltpu.VMEM((rows, 1), f32),
-            pltpu.VMEM((rows, tile), f32),
-            pltpu.VMEM((rows, 1), f32),
-            pltpu.VMEM((rows, 1), f32),
-            pltpu.VMEM((rows, tile), f32),
+            pltpu.VMEM((rows, latent_size + tile), bf16),
+            pltpu.VMEM((n_sp, rows, latent_size + tile), bf16),
+            pltpu.VMEM((latent_size, 4 * tile), bf16),
+            pltpu.VMEM((3, rows, tile), bf16),
+            pltpu.VMEM((2, rows, n_sp * rows), f32),
+            pltpu.VMEM((n_sp * rows, 2 * tile), bf16),
             pltpu.VMEM((rows, width), bf16),
             pltpu.VMEM((n_tp - 1, tok_count, width), bf16),
-        ]
-        + [dma((n_sp - 1,))] * 8
-        + [dma((n_tp - 1,))] * 2,
-        compiler_params=pltpu.CompilerParams(
-            collective_id=0, has_side_effects=True, vmem_limit_bytes=24 * 2**20
-        ),
-    )(pack, qs, ql, proj, small_output, large_output, residual)
-    return pl.pallas_call(
-        functools.partial(expert_kernel, n_sp, n_tp, capacity),
-        name="experts",
-        out_shape=jax.ShapeDtypeStruct(residual.shape, bf16),
-        in_specs=[in_vmem] * 4 + [in_hbm] * 3,
-        out_specs=in_vmem,
-        scratch_shapes=[
+            pltpu.VMEM((tok_count, width), bf16),
             pltpu.VMEM((width, hidden_units), bf16),
             pltpu.VMEM((width, hidden_units), bf16),
             pltpu.VMEM((hidden_units, width), bf16),
@@ -765,19 +773,34 @@
             pltpu.VMEM((slots, width), bf16),
             pltpu.VMEM((slots, width), bf16),
             pltpu.VMEM((slots, width), bf16),
-            dma((3,)),
         ]
+        + [dma((n_sp - 1,))] * 8
+        + [dma((n_tp - 1,))] * 2
+        + [dma((3,))]
         + [dma((n_sp,))] * 8
         + [dma((2,))] * 2
         + [dma((n_sp,))] * 4,
         compiler_params=pltpu.CompilerParams(
-            collective_id=1, has_side_effects=True, vmem_limit_bytes=48 * 2**20
+            collective_id=0, has_side_effects=True, vmem_limit_bytes=60 * 2**20
         ),
     )(
-        middle,
+        latent,
+        rotary_key.T,
+        latent_gain.reshape(1, latent_size),
+        cos_table,
+        sin_table,
+        query_small.T,
+        query_large.T,
+        small_keys.T,
+        small_values.T,
+        large_keys,
+        large_values,
+        small_output,
+        large_output,
+        residual,
         ffn_gain.reshape(1, width),
-        routing,
-        route_weight,
+        routing.T,
+        route_weight.T,
         gate_weights,
         up_weights,
         down_weights,
@@ -796,6 +819,7 @@
         and capacity % 16 == 0
         and n_sp * capacity % 128 == 0
         and tok_count % 16 == 0
+        and latent.shape[0] % 128 == 0
         and args[6].shape[1] == NOPE_S
         and args[8].shape[1] == NOPE_L
     )

time: 89.9 us -> 76.7 us (0.85); the launches traced: 88.3 us -> 76.5 us
  other arithmetic: 4.86 us -> 0 us
  local copies, waits for them, and re-layouts: 5.49 us -> 1.57 us
  Pallas kernels: 77.7 us -> 75 us
    unnamed x25 -> x1, local copies, waits for them, and re-layouts: 5.34 us -> 1.57 us
    pallas_call x2 -> x1, Pallas kernels: 77.7 us -> 75 us  [in_kernels(): pl.pallas_call(functools.partial(layer_kernel, n_sp, n_tp, capacity), nam...]
    convert_element_type x4 -> x0, other arithmetic: 1.95 us -> none  [the longest x1 1.01 us: in_kernels(): rms_scaled(latent, latent_gain).astype(jnp.bfloat16)]
    concatenate x4 -> x0, other arithmetic: 1.24 us -> none  [the longest x1 1.07 us: in_kernels(): jnp.concatenate([jnp.pad(small_keys, ((0, 0), (0, tile - small_keys.shape...]
    reduce_sum x1 -> x0, other arithmetic: 1.02 us -> none  [rms_scaled(): jnp.mean(widened * widened, axis=-1, keepdims=True) + eps]
where the time goes in v2:
time: 76.7 us; the launch traced here: 76.5 us
  Pallas kernels  75 us (98%)
  local copies, waits for them, and re-layouts  1.57 us (2%)
    pallas_call x1, Pallas kernels, in_kernels(): pl.pallas_call(functools.partial(layer_kernel, n_sp, n_tp, capacity), nam...  75 us
    unnamed x1, local copies, waits for them, and re-layouts  1.57 us

profile of v2, /device:TPU:0, one launch (start us, length us, event | category | flops | bytes accessed | tf_op | source)
XLA Modules:
  0.0 76.5 jit_solution(16707068562611622254)
XLA Ops:
  0.0 75.0 %layer.1 = bf16[32,2048]{1,0:T(8,128)(2,1)} custom-call(bf16[128,512]{1,0:T(8,128)(2,1)} %latent_ref.1, bf16[32,128]{1,0:T(8,128)(2,1)} %bitcast.13, f32[1,512]{1,0:T(1,128)} %bitcast.15, f32[16,1024]{1,0:T(8,128)} %constant.4.clone.cos_ref, f32[16,1024]{1,0:T(8,128)} %constant.5.clone.sin_ref, bf16[96,128]{1,0:T(8,128)(2,1)} %bitcast.12, ...), custom_call_target="tpu_custom_call" | custom-call | tf_op jit(solution)/shard_map/layer/pallas_call | solution.py:749
  75.0 1.6 %copy.22 = bf16[32,2048]{1,0:T(8,128)(2,1)} copy(bf16[32,2048]{1,0:T(8,128)(2,1)} %layer.1) | data formatting | bytes 262144
